TPU v7x, 32 devices: a whole 2x2x4 slice. The times are simulated.
32 devices in a mesh: grp: 2 (over y), sp: 4 (over z), tp: 4 (over x, core).
Axes of the slice: x: 2, y: 2, z: 4, core: 2. Of those that a mesh axis runs over, the one named last changes fastest.
Arguments:
- resid_in: bfloat16 [2048, 2048], P(('grp', 'sp', 'tp')), parts along dimension 0, may hold values from -3 to 3
- queries: bfloat16 [2048, 1024], P(('grp', 'sp'), 'tp'), parts along dimension 0, may hold values from -39 to 39
- keys: bfloat16 [2048, 1024], P(('grp', 'sp'), 'tp'), parts along dimension 0, may hold values from -6 to 6
- values: bfloat16 [2048, 1024], P(('grp', 'sp'), 'tp'), parts along dimension 0, may hold values from -12 to 12
- cum_gate: float32 [2048, 16], P('grp', 'tp'), parts along dimension 0, may hold values from -105 to 0, as said below
- w_out: bfloat16 [1024, 2048], replicated, may hold values from -0.1875 to 0.1875
- norm_gain: float32 [2048], replicated, may hold values from 0.1 to 1.9
- w_gate: bfloat16 [2048, 5632], P('sp', 'tp'), may hold values from -0.125 to 0.125
- w_up: bfloat16 [2048, 5632], P('sp', 'tp'), may hold values from -0.125 to 0.125
- w_down: bfloat16 [5632, 2048], P('tp', 'sp'), may hold values from -0.078125 to 0.078125
Outputs:
- resid_out: bfloat16 [2048, 2048], P(('grp', 'sp', 'tp')), parts along dimension 0
There are 2 independent parts, one for each index of `grp`. A program takes and returns all parts, laid end to end along the dimension named above; an argument that names none is the same for every part. Nothing has to cross between parts.
Inputs may be any that keep to these rules, and one draw needn't show every extreme that they name: `cum_gate`: in every head the values never rise from one position to the next, and the first is at most 0.
All inputs are finite; a program needn't handle non-finite values.
Results may differ from a plain program's by a relative error of at most 0.018.
Values may be sent and summed in bfloat16 or wider, within the bound.
A program may use at most 128 MiB of HBM per device.

v0:
```python
import math

import jax
import jax.numpy as jnp
from jax import lax
from jax.sharding import PartitionSpec as P

HEAD_DIM = 64


def on_device(resid_in, queries, keys, values, cum_gate, w_out, norm_gain, w_gate, w_up, w_down):
    tok_rows = queries.shape[0]
    local_heads = queries.shape[1] // HEAD_DIM
    scale = HEAD_DIM ** (-0.5)
    offset = lax.axis_index("sp") * tok_rows
    query_heads = queries.reshape(tok_rows, local_heads, HEAD_DIM)
    own_gate = lax.dynamic_slice_in_dim(cum_gate, offset, tok_rows, 0).T
    query_pos = offset + jnp.arange(tok_rows, dtype=jnp.int32)
    last_pos = offset + tok_rows - 1
    initial = (
        jnp.full((local_heads, tok_rows), -1e30, jnp.float32),
        jnp.zeros((local_heads, tok_rows), jnp.float32),
        jnp.zeros((tok_rows, local_heads, HEAD_DIM), jnp.float32),
    )
    key_piece = lax.all_gather(keys, "sp", axis=0, tiled=True)
    value_piece = lax.all_gather(values, "sp", axis=0, tiled=True)
    length = key_piece.shape[0]
    span = math.gcd(length, 512)

    def block(index, state):
        begin = index * span

        def work(inner):
            maxima, totals, summed = inner
            key_block = lax.dynamic_slice_in_dim(key_piece, index * span, span, 0).reshape(
                span, local_heads, HEAD_DIM
            )
            value_block_rows = lax.dynamic_slice_in_dim(value_piece, index * span, span, 0).reshape(
                span, local_heads, HEAD_DIM
            )
            key_gate = lax.dynamic_slice_in_dim(cum_gate, begin, span, 0).T
            scores = (
                jnp.einsum(
                    "qhd,khd->hqk", query_heads, key_block, preferred_element_type=jnp.float32
                )
                * scale
            )
            scores = scores + own_gate[:, :, None] - key_gate[:, None, :]
            key_pos = begin + jnp.arange(span, dtype=jnp.int32)
            mask = (key_pos[None, :] <= query_pos[:, None])[None]
            scores = jnp.where(mask, scores, -1e30)
            new_max = jnp.maximum(maxima, jnp.max(scores, axis=-1))
            weights = jnp.where(mask, jnp.exp(scores - new_max[:, :, None]), 0.0)
            rescale = jnp.exp(maxima - new_max)
            totals = totals * rescale + jnp.sum(weights, axis=-1)
            product = jnp.einsum(
                "hqk,khd->qhd",
                weights.astype(jnp.bfloat16),
                value_block_rows,
                preferred_element_type=jnp.float32,
            )
            summed = summed * rescale.T[:, :, None] + product
            return (new_max, totals, summed)

        return lax.cond(begin <= last_pos, work, lambda inner: inner, state)

    maxima, totals, summed = lax.fori_loop(0, length // span, block, initial)
    attended = (
        (summed / totals.T[:, :, None])
        .reshape(tok_rows, local_heads * HEAD_DIM)
        .astype(jnp.bfloat16)
    )
    head_rows = lax.all_to_all(attended, "tp", split_axis=0, concat_axis=1, tiled=True)
    mixed = jnp.dot(head_rows, w_out, preferred_element_type=jnp.float32)
    resid = resid_in.astype(jnp.float32) + mixed
    normed = resid * lax.rsqrt(jnp.mean(resid * resid, axis=-1, keepdims=True) + 1e-06)
    normed = (normed * norm_gain).astype(jnp.bfloat16)
    all_rows = lax.all_gather(normed, "tp", axis=0, tiled=True)
    full_gate, full_up, full_down = (
        lax.all_gather(w_gate, "sp", axis=0, tiled=True),
        lax.all_gather(w_up, "sp", axis=0, tiled=True),
        lax.all_gather(w_down, "sp", axis=1, tiled=True),
    )
    gate = jnp.dot(all_rows, full_gate, preferred_element_type=jnp.float32)
    up = jnp.dot(all_rows, full_up, preferred_element_type=jnp.float32)
    hidden = (jax.nn.silu(gate) * up).astype(jnp.bfloat16)
    terms = jnp.dot(hidden, full_down, preferred_element_type=jnp.float32)
    back = lax.psum_scatter(
        terms.astype(jnp.bfloat16), "tp", scatter_dimension=0, tiled=True
    ).astype(jnp.float32)
    return (resid + back).astype(jnp.bfloat16)


def solution(mesh):
    return jax.shard_map(
        on_device,
        mesh=mesh,
        in_specs=(
            P(("grp", "sp", "tp"), None),
            P(("grp", "sp"), "tp"),
            P(("grp", "sp"), "tp"),
            P(("grp", "sp"), "tp"),
            P("grp", "tp"),
            P(),
            P(),
            P("sp", "tp"),
            P("sp", "tp"),
            P("tp", "sp"),
        ),
        out_specs=P(("grp", "sp", "tp"), None),
        check_vma=False,
    )
```

profile of v0, /device:TPU:0, one launch (start us, length us, event | category | flops | bytes accessed | tf_op | source)
XLA Modules:
  0.0 436.8 jit_solution(10608171273558845246)
XLA Ops:
  6.5 0.0 copy-start.1
  6.5 0.0 all-gather.5.cloned.1.call-start
  6.5 1.0 copy.16
  7.6 17.4 %all_gather.18 = bf16[1024,256]{0,1:T(8,128)(2,1)S(1)} all-gather(bf16[256,256]{0,1:T(8,128)(2,1)S(1)} %copy.16), channel_id=1, replica_groups=mesh['grp'=2,'sp'=4,'tp'=4] {'sp'}, dimensions={0}, use_global_device_ids=true | all-gather | bytes 655360 | tf_op jit(solution)/shard_map/all_gather | solution.py:25
  24.9 1.0 copy.18
  25.9 16.3 %all_gather.19 = bf16[1024,256]{0,1:T(8,128)(2,1)S(1)} all-gather(bf16[256,256]{0,1:T(8,128)(2,1)S(1)} %copy.18), channel_id=1, replica_groups=mesh['grp'=2,'sp'=4,'tp'=4] {'sp'}, dimensions={0}, use_global_device_ids=true | all-gather | bytes 655360 | tf_op jit(solution)/shard_map/all_gather | solution.py:26
  42.2 1.0 copy.17
  43.2 0.0 copy-done.1
  43.3 0.0 copy-start
  43.3 2.1 while.18
  43.3 2.0 conditional.3
  43.4 0.1 broadcast_compare_fusion
  43.6 0.7 fusion.13
  44.3 0.5 fusion.4
  44.9 0.4 fusion.3
  45.4 0.2 reshape.60
  45.6 0.2 copy.22
  45.7 7.2 %all_to_all.16 = bf16[4,64,256]{2,1,0:T(8,128)(2,1)S(1)} all-to-all(bf16[4,64,256]{2,1,0:T(8,128)(2,1)S(1)} %copy.22), channel_id=1, replica_groups=mesh['grp'=2,'sp'=4,'tp'=4] {'tp'}, dimensions={0} | all-to-all | bytes 262144 | tf_op jit(solution)/shard_map/all_to_all | solution.py:73
  52.9 0.0 copy-done
  52.9 0.0 copy-start.2
  52.9 3.2 multiply_reduce_fusion
  56.1 0.0 copy-done.2
  56.1 0.8 multiply_convert_fusion
  56.9 0.0 all-gather.5.cloned.1.call-update
  57.0 0.0 all-gather.7.cloned.1.call-start
  57.0 0.7 all-gather.7.cloned.1.call-update
  57.7 0.0 all-gather.11.cloned.1.call-start
  57.8 0.7 all-gather.11.cloned.1.call-update
  58.5 0.0 all-gather.9.cloned.1.call-start
  58.5 0.5 all-gather.9.cloned.1.call-update
  59.0 0.0 reduce-scatter.2.cloned.1.call-start
  59.1 16.3 %all-gather.5.cloned.1.call-done = bf16[256,2048]{1,0:T(8,128)(2,1)} async-done(((bf16[64,2048]{1,0:T(8,128)(2,1)}), bf16[256,2048]{1,0:T(8,128)(2,1)}) %all-gather.5.cloned.1.call-update) | async-done | bytes 1048592 | tf_op jit(solution)/shard_map/all_gather | solution.py:78
  75.3 0.0 copy-start.3
  75.3 108.3 %all-gather.7.cloned.1.call-done = bf16[2048,1408]{1,0:T(8,128)(2,1)} async-done(((bf16[512,1408]{1,0:T(8,128)(2,1)}), bf16[2048,1408]{1,0:T(8,128)(2,1)}) %all-gather.7.cloned.1.call-update) | async-done | bytes 5767184 | tf_op jit(solution)/shard_map/all_gather | solution.py:80
  183.6 4.8 %fusion.14 = f32[256,1408]{1,0:T(8,128)S(1)} fusion(bf16[256,2048]{1,0:T(8,128)(2,1)} %all-gather.5.cloned.1.call-done, bf16[2048,1408]{1,0:T(8,128)(2,1)} %all-gather.7.cloned.1.call-done), kind=kOutput, calls=%fused_computation.32 | convolution fusion | flops 1476395008 | bytes 8257536 | tf_op jit(solution)/shard_map/dot_general | solution.py:84
  188.4 101.8 %all-gather.11.cloned.1.call-done = bf16[1408,2048]{1,0:T(8,128)(2,1)} async-done(((bf16[1408,512]{1,0:T(8,128)(2,1)}), bf16[1408,2048]{1,0:T(8,128)(2,1)}) %all-gather.11.cloned.1.call-update) | async-done | bytes 5767184 | tf_op jit(solution)/shard_map/all_gather | solution.py:82
  290.2 106.4 %all-gather.9.cloned.1.call-done = bf16[2048,1408]{1,0:T(8,128)(2,1)} async-done(((bf16[512,1408]{1,0:T(8,128)(2,1)}), bf16[2048,1408]{1,0:T(8,128)(2,1)}) %all-gather.9.cloned.1.call-update) | async-done | bytes 5767184 | tf_op jit(solution)/shard_map/all_gather | solution.py:81
  396.6 0.0 copy-done.3
  396.6 8.8 %convolution_convert_fusion = bf16[256,2048]{1,0:T(8,128)(2,1)} fusion(bf16[1408,2048]{1,0:T(8,128)(2,1)} %all-gather.11.cloned.1.call-done, bf16[256,2048]{1,0:T(8,128)(2,1)S(1)} %copy-done.3, bf16[2048,1408]{1,0:T(8,128)(2,1)} %all-gather.9.cloned.1.call-done, f32[256,1408]{1,0:T(8,128)S(1)} %fusion.14), kind=kOutput, calls=%fused_computation.22 | convolution fusion | flops 2955476992 | bytes 15073280 | tf_op jit(solution)/shard_map/dot_general | solution.py:87
  405.4 0.0 reduce-scatter.2.cloned.1.call-update
  405.4 23.2 %reduce-scatter.2.cloned.1.call-done = bf16[64,2048]{1,0:T(8,128)(2,1)} async-done(((bf16[256,2048]{1,0:T(8,128)(2,1)}), bf16[64,2048]{1,0:T(8,128)(2,1)}) %reduce-scatter.2.cloned.1.call-update) | async-done | bytes 262160 | tf_op jit(solution)/shard_map/reduce_scatter | solution.py:88
  428.6 1.7 add_convert_fusion
  (17 shorter events, 0.2 us)
Async XLA Ops:
  6.5 36.7 %copy-start.1 = (f32[1024,4]{0,1:T(4,128)S(1)}, f32[1024,4]{0,1:T(4,128)}, u32[]{:S(2)}) copy-start(f32[1024,4]{0,1:T(4,128)} %param.18) | copy-start | bytes 49156
  6.5 68.8 %all-gather.5.cloned.1.call-start = ((), (), s32[]{:S(2)}) async-start(), calls=%async_computation.2 | async-start | bytes 1310720 | tf_op jit(solution)/shard_map/all_gather | solution.py:78
  43.3 9.6 %copy-start = (bf16[64,2048]{1,0:T(8,128)(2,1)S(1)}, bf16[64,2048]{1,0:T(8,128)(2,1)}, u32[]{:S(2)}) copy-start(bf16[64,2048]{1,0:T(8,128)(2,1)} %param.14) | copy-start | bytes 786436
  52.9 3.2 copy-start.2
  57.0 126.7 %all-gather.7.cloned.1.call-start = ((), (), s32[]{:S(2)}) async-start(), calls=%async_computation.3 | async-start | bytes 7208960 | tf_op jit(solution)/shard_map/all_gather | solution.py:80
  57.7 232.5 %all-gather.11.cloned.1.call-start = ((), (), s32[]{:S(2)}) async-start(), calls=%async_computation.5 | async-start | bytes 7208960 | tf_op jit(solution)/shard_map/all_gather | solution.py:82
  58.5 338.1 %all-gather.9.cloned.1.call-start = ((), (), s32[]{:S(2)}) async-start(), calls=%async_computation.4 | async-start | bytes 7208960 | tf_op jit(solution)/shard_map/all_gather | solution.py:81
  59.0 369.6 %reduce-scatter.2.cloned.1.call-start = ((), (), s32[]{:S(2)}) async-start(), calls=%async_computation.6 | async-start | bytes 1310720 | tf_op jit(solution)/shard_map/reduce_scatter | solution.py:88
  75.3 321.2 %copy-start.3 = (bf16[256,2048]{1,0:T(8,128)(2,1)S(1)}, bf16[256,2048]{1,0:T(8,128)(2,1)}, u32[]{:S(2)}) copy-start(bf16[256,2048]{1,0:T(8,128)(2,1)} %all-gather.5.cloned.1.call-done) | copy-start | bytes 3145732
Sparse Core Ops, SparseCore 0:
  57.1 18.2 all-gather.4
  76.9 106.6 all-gather.6
  185.2 104.9 all-gather.10
  291.6 104.9 all-gather.8
  405.5 23.0 reduce-scatter.1
where the time goes:
time: 437 us
  waiting for transfers between devices  358 us (82%)
  blocking collectives  40.8 us (9%)
  matrix products  18 us (4%)
  between operations  13.3 us (3%)
    all_gather x1, waiting for transfers between devices, on_device(): lax.all_gather(w_gate, 'sp', axis=0, tiled=True)  108 us
    all_gather x1, waiting for transfers between devices, on_device(): lax.all_gather(w_up, 'sp', axis=0, tiled=True)  106 us
    all_gather x1, waiting for transfers between devices, on_device(): lax.all_gather(w_down, 'sp', axis=1, tiled=True)  102 us
    reduce_scatter x1, waiting for transfers between devices, on_device(): lax.psum_scatter(terms.astype(jnp.bfloat16), 'tp', scatter_dimension=0, t...  23.2 us
    all_gather x1, blocking collectives, on_device(): key_piece = lax.all_gather(keys, 'sp', axis=0, tiled=True)  17.4 us
    all_gather x1, waiting for transfers between devices, on_device(): all_rows = lax.all_gather(normed, 'tp', axis=0, tiled=True)  16.3 us
    all_gather x1, blocking collectives, on_device(): value_piece = lax.all_gather(values, 'sp', axis=0, tiled=True)  16.3 us
    dot_general x1, matrix products, on_device(): terms = jnp.dot(hidden, full_down, preferred_element_type=jnp.float32)  8.81 us
  transfers between devices with their start and end apart: 5, of which 5 were waited for; matrix products, arithmetic and copies ran while one was open for 1% of the time, Pallas kernels for 0%

commit v1 on v0

--- a/solution.py
+++ b/solution.py
@@ -22,8 +22,8 @@
         jnp.zeros((local_heads, tok_rows), jnp.float32),
         jnp.zeros((tok_rows, local_heads, HEAD_DIM), jnp.float32),
     )
-    key_piece = lax.all_gather(keys, "sp", axis=0, tiled=True)
-    value_piece = lax.all_gather(values, "sp", axis=0, tiled=True)
+    pair = lax.all_gather(jnp.stack([keys, values]), "sp", axis=1, tiled=True)
+    key_piece, value_piece = pair[0], pair[1]
     length = key_piece.shape[0]
     span = math.gcd(length, 512)
 
@@ -75,18 +75,18 @@
     resid = resid_in.astype(jnp.float32) + mixed
     normed = resid * lax.rsqrt(jnp.mean(resid * resid, axis=-1, keepdims=True) + 1e-06)
     normed = (normed * norm_gain).astype(jnp.bfloat16)
-    all_rows = lax.all_gather(normed, "tp", axis=0, tiled=True)
+    all_rows = lax.all_gather(normed, ("sp", "tp"), axis=0, tiled=True)
     full_gate, full_up, full_down = (
-        lax.all_gather(w_gate, "sp", axis=0, tiled=True),
-        lax.all_gather(w_up, "sp", axis=0, tiled=True),
-        lax.all_gather(w_down, "sp", axis=1, tiled=True),
+        lax.all_to_all(w_gate, "sp", split_axis=1, concat_axis=0, tiled=True),
+        lax.all_to_all(w_up, "sp", split_axis=1, concat_axis=0, tiled=True),
+        lax.all_to_all(w_down, "sp", split_axis=0, concat_axis=1, tiled=True),
     )
     gate = jnp.dot(all_rows, full_gate, preferred_element_type=jnp.float32)
     up = jnp.dot(all_rows, full_up, preferred_element_type=jnp.float32)
     hidden = (jax.nn.silu(gate) * up).astype(jnp.bfloat16)
     terms = jnp.dot(hidden, full_down, preferred_element_type=jnp.float32)
     back = lax.psum_scatter(
-        terms.astype(jnp.bfloat16), "tp", scatter_dimension=0, tiled=True
+        terms.astype(jnp.bfloat16), ("sp", "tp"), scatter_dimension=0, tiled=True
     ).astype(jnp.float32)
     return (resid + back).astype(jnp.bfloat16)
 

time: 437 us -> 288 us (0.66)
  waiting for transfers between devices: 358 us -> 217 us
  blocking collectives: 40.8 us -> 6.99 us
  starting transfers between devices: 0.16 us -> 12.6 us
  local copies, waits for them, and re-layouts: 3.45 us -> 15 us
    all_gather x4 -> x2, waiting for transfers between devices: 333 us -> 31 us  [the longest x1 31 us: on_device(): pair = lax.all_gather(jnp.stack([keys, values]), 'sp', axis=1, tiled=True)]
    all_to_all x0 -> x3, waiting for transfers between devices: none -> 114 us  [the longest x1 41.6 us: on_device(): lax.all_to_all(w_gate, 'sp', split_axis=1, concat_axis=0, tiled=True)]
    reduce_scatter x1, waiting for transfers between devices: 23.2 us -> 72 us  [on_device(): lax.psum_scatter(terms.astype(jnp.bfloat16), ('sp', 'tp'), scatter_dimens...]
    all_gather x2 -> x0, blocking collectives: 33.6 us -> none  [the longest x1 17.4 us: on_device(): key_piece = lax.all_gather(keys, 'sp', axis=0, tiled=True)]
    all_to_all x0 -> x3, starting transfers between devices: none -> 12.6 us  [the longest x1 4.41 us: on_device(): lax.all_to_all(w_gate, 'sp', split_axis=1, concat_axis=0, tiled=True)]
    all_to_all x0 -> x3, local copies, waits for them, and re-layouts: none -> 5.37 us  [the longest x1 2.72 us: on_device(): lax.all_to_all(w_up, 'sp', split_axis=1, concat_axis=0, tiled=True)]
  transfers between devices with their start and end apart: 5 -> 6, of which waited for: 5 -> 5; matrix products, arithmetic and copies ran while one was open for 1% -> 4% of each run, Pallas kernels for 0% -> 0%
where the time goes in v1:
time: 288 us
  waiting for transfers between devices  217 us (75%)
  matrix products  18.5 us (6%)
  local copies, waits for them, and re-layouts  15 us (5%)
  between operations  13.3 us (5%)
  starting transfers between devices  12.6 us (4%)
  blocking collectives  6.99 us (2%)
  other arithmetic  3.84 us (1%)
    reduce_scatter x1, waiting for transfers between devices, on_device(): lax.psum_scatter(terms.astype(jnp.bfloat16), ('sp', 'tp'), scatter_dimens...  72 us
    all_to_all x1, waiting for transfers between devices, on_device(): lax.all_to_all(w_gate, 'sp', split_axis=1, concat_axis=0, tiled=True)  41.6 us
    all_to_all x1, waiting for transfers between devices, on_device(): lax.all_to_all(w_down, 'sp', split_axis=0, concat_axis=1, tiled=True)  40.6 us
    all_to_all x1, waiting for transfers between devices, on_device(): lax.all_to_all(w_up, 'sp', split_axis=1, concat_axis=0, tiled=True)  31.8 us
    all_gather x1, waiting for transfers between devices, on_device(): pair = lax.all_gather(jnp.stack([keys, values]), 'sp', axis=1, tiled=True)  31 us
    dot_general x1, matrix products, on_device(): terms = jnp.dot(hidden, full_down, preferred_element_type=jnp.float32)  9 us
    unnamed x17, local copies, waits for them, and re-layouts  7.24 us
    all_to_all x1, blocking collectives, on_device(): lax.all_to_all(attended, 'tp', split_axis=0, concat_axis=1, tiled=True)  6.99 us
  transfers between devices with their start and end apart: 6, of which 5 were waited for; matrix products, arithmetic and copies ran while one was open for 4% of the time, Pallas kernels for 0%

profile of v1, /device:TPU:0, one launch (start us, length us, event | category | flops | bytes accessed | tf_op | source)
XLA Modules:
  0.0 287.6 jit_solution(10348079197121821189)
XLA Ops:
  6.5 0.0 copy-start.4
  6.5 0.0 all-gather.3.cloned.1.call-start
  6.5 1.0 copy.27
  7.6 1.0 copy.28
  8.6 0.7 pad_maximum_fusion
  9.3 0.0 all-gather.3.cloned.1.call-update
  9.3 0.0 all-gather.5.cloned.1.call-start
  9.4 1.0 copy.29
  10.4 0.7 dynamic-slice_bitcast_fusion.1
  11.1 31.0 %all-gather.3.cloned.1.call-done = bf16[2,1024,256]{1,2,0:T(8,128)(2,1)} async-done(((bf16[2,256,256]{1,2,0:T(8,128)(2,1)}), bf16[2,1024,256]{1,2,0:T(8,128)(2,1)}) %all-gather.3.cloned.1.call-update) | async-done | bytes 1048592 | tf_op jit(solution)/shard_map/all_gather | solution.py:25
  42.1 1.3 slice_bitcast_fusion
  43.4 0.0 copy-done.4
  43.5 0.0 copy-start.3
  43.5 2.1 while.18
  43.5 2.0 conditional.3
  43.6 0.1 broadcast_compare_fusion
  43.8 0.7 fusion.14
  44.5 0.5 fusion.4
  45.1 0.4 fusion.3
  45.6 0.2 reshape.69
  45.8 0.2 copy.38
  45.9 7.0 %all_to_all.73 = bf16[4,64,256]{2,1,0:T(8,128)(2,1)S(1)} all-to-all(bf16[4,64,256]{2,1,0:T(8,128)(2,1)S(1)} %copy.38), channel_id=1, replica_groups=mesh['grp'=2,'sp'=4,'tp'=4] {'tp'}, dimensions={0} | all-to-all | bytes 262144 | tf_op jit(solution)/shard_map/all_to_all | solution.py:73
  52.9 0.0 copy-done.3
  53.0 0.0 copy-start.5
  53.0 3.2 %multiply_reduce_fusion = (f32[64]{0:T(128)S(1)}, f32[64,2048]{1,0:T(8,128)S(1)}) fusion(bf16[64,1024]{1,0:T(8,128)(2,1)S(1)} %bitcast.62, bf16[1024,2048]{1,0:T(8,128)(2,1)} %param.19, bf16[64,2048]{1,0:T(8,128)(2,1)S(1)} %copy-done.3), kind=kOutput, calls=%fused_computation.29 | convolution fusion | flops 268959680 | bytes 5112064 | tf_op jit(solution)/shard_map/dot_general | solution.py:74
  56.1 0.0 copy-start
  56.2 0.0 copy-done.5
  56.2 0.8 multiply_convert_fusion
  57.0 0.0 all-gather.5.cloned.1.call-update
  57.0 3.8 %all-to-all-start.3 = ((bf16[4,352,512]{2,1,0:T(8,128)(2,1)}), bf16[4,352,512]{2,1,0:T(8,128)(2,1)S(1)}, u32[]{:S(2)}, u32[]{:S(2)}) async-start(bf16[4,352,512]{2,1,0:T(8,128)(2,1)} %bitcast.55), calls=%async_computation.3 | async-start | bytes 2883584 | tf_op jit(solution)/shard_map/all_to_all | solution.py:82
  60.8 0.0 copy-done
  60.8 1.6 copy.32
  62.4 40.6 %all-to-all-done.3 = bf16[4,352,512]{2,1,0:T(8,128)(2,1)S(1)} async-done(((bf16[4,352,512]{2,1,0:T(8,128)(2,1)}), bf16[4,352,512]{2,1,0:T(8,128)(2,1)S(1)}, u32[]{:S(2)}, u32[]{:S(2)}) %all-to-all-start.3) | async-done | bytes 1441824 | tf_op jit(solution)/shard_map/all_to_all | solution.py:82
  103.0 4.4 %all-to-all-start.1 = ((bf16[512,4,352]{0,2,1:T(8,128)(2,1)}), bf16[512,4,352]{0,2,1:T(8,128)(2,1)S(1)}, u32[]{:S(2)}, u32[]{:S(2)}) async-start(bf16[512,4,352]{0,2,1:T(8,128)(2,1)} %bitcast.54), calls=%async_computation.1 | async-start | bytes 2883584 | tf_op jit(solution)/shard_map/all_to_all | solution.py:80
  107.4 2.6 copy.34
  110.1 41.6 %all-to-all-done.1 = bf16[512,4,352]{0,2,1:T(8,128)(2,1)S(1)} async-done(((bf16[512,4,352]{0,2,1:T(8,128)(2,1)}), bf16[512,4,352]{0,2,1:T(8,128)(2,1)S(1)}, u32[]{:S(2)}, u32[]{:S(2)}) %all-to-all-start.1) | async-done | bytes 1441824 | tf_op jit(solution)/shard_map/all_to_all | solution.py:80
  151.7 4.3 %all-to-all-start.2 = ((bf16[512,4,352]{0,2,1:T(8,128)(2,1)}), bf16[512,4,352]{0,2,1:T(8,128)(2,1)}, u32[]{:S(2)}, u32[]{:S(2)}) async-start(bf16[512,4,352]{0,2,1:T(8,128)(2,1)} %bitcast.53), calls=%async_computation.2 | async-start | bytes 2883584 | tf_op jit(solution)/shard_map/all_to_all | solution.py:81
  156.0 0.0 reduce-scatter.2.cloned.1.call-start
  156.1 1.3 copy.42
  157.4 1.3 copy.40
  158.7 0.0 copy-start.2
  158.7 31.8 %all-to-all-done.2 = bf16[512,4,352]{0,2,1:T(8,128)(2,1)} async-done(((bf16[512,4,352]{0,2,1:T(8,128)(2,1)}), bf16[512,4,352]{0,2,1:T(8,128)(2,1)}, u32[]{:S(2)}, u32[]{:S(2)}) %all-to-all-start.2) | async-done | bytes 1441824 | tf_op jit(solution)/shard_map/all_to_all | solution.py:81
  190.5 2.7 copy.41
  193.2 0.0 all-gather.5.cloned.1.call-done
  193.2 0.0 copy-done.2
  193.2 0.0 copy-start.1
  193.2 5.1 %fusion.15 = f32[1024,352]{0,1:T(8,128)} fusion(bf16[1024,2048]{1,0:T(8,128)(2,1)} %all-gather.5.cloned.1.call-done, bf16[2048,352]{0,1:T(8,128)(2,1)S(1)} %bitcast.57), kind=kOutput, calls=%fused_computation.36 | convolution fusion | flops 1476395008 | bytes 7077888 | tf_op jit(solution)/shard_map/dot_general | solution.py:84
  198.3 0.0 copy-done.1
  198.3 9.0 %convolution_convert_fusion = bf16[1024,2048]{1,0:T(8,128)(2,1)} fusion(bf16[352,2048]{1,0:T(8,128)(2,1)S(1)} %bitcast.56, bf16[1024,2048]{1,0:T(8,128)(2,1)} %all-gather.5.cloned.1.call-done, bf16[2048,352]{0,1:T(8,128)(2,1)} %bitcast.58, f32[1024,352]{0,1:T(8,128)} %fusion.15), kind=kOutput, calls=%fused_computation.20 | convolution fusion | flops 2957049856 | bytes 12713984 | tf_op jit(solution)/shard_map/dot_general | solution.py:87
  207.3 0.0 reduce-scatter.2.cloned.1.call-update
  207.3 72.0 %reduce-scatter.2.cloned.1.call-done = bf16[64,2048]{1,0:T(8,128)(2,1)} async-done(((bf16[1024,2048]{1,0:T(8,128)(2,1)}), bf16[64,2048]{1,0:T(8,128)(2,1)}) %reduce-scatter.2.cloned.1.call-update) | async-done | bytes 262160 | tf_op jit(solution)/shard_map/reduce_scatter | solution.py:88
  279.4 1.7 add_convert_fusion
  (16 shorter events, 0.2 us)
Async XLA Ops:
  6.5 36.9 %copy-start.4 = (f32[1024,4]{0,1:T(4,128)S(1)}, f32[1024,4]{0,1:T(4,128)}, u32[]{:S(2)}) copy-start(f32[1024,4]{0,1:T(4,128)} %param.18) | copy-start | bytes 49156
  6.5 35.6 %all-gather.3.cloned.1.call-start = ((), (), s32[]{:S(2)}) async-start(), calls=%async_computation.5 | async-start | bytes 1310720 | tf_op jit(solution)/shard_map/all_gather | solution.py:25
  9.3 183.9 %all-gather.5.cloned.1.call-start = ((), (), s32[]{:S(2)}) async-start(), calls=%async_computation.6 | async-start | bytes 4456448 | tf_op jit(solution)/shard_map/all_gather | solution.py:78
  43.5 9.5 %copy-start.3 = (bf16[64,2048]{1,0:T(8,128)(2,1)S(1)}, bf16[64,2048]{1,0:T(8,128)(2,1)}, u32[]{:S(2)}) copy-start(bf16[64,2048]{1,0:T(8,128)(2,1)} %param.14) | copy-start | bytes 786436
  53.0 3.2 %copy-start.5 = (f32[2048]{0:T(1024)S(1)}, f32[2048]{0:T(1024)}, u32[]{:S(2)}) copy-start(f32[2048]{0:T(1024)} %param.20) | copy-start | bytes 24580
  56.1 4.7 %copy-start = (bf16[512,1408]{1,0:T(8,128)(2,1)S(1)}, bf16[512,1408]{1,0:T(8,128)(2,1)}, u32[]{:S(2)}) copy-start(bf16[512,1408]{1,0:T(8,128)(2,1)} %param.21) | copy-start | bytes 4325380
  57.0 46.0 %all-to-all-start.3 = ((bf16[4,352,512]{2,1,0:T(8,128)(2,1)}), bf16[4,352,512]{2,1,0:T(8,128)(2,1)S(1)}, u32[]{:S(2)}, u32[]{:S(2)}) async-start(bf16[4,352,512]{2,1,0:T(8,128)(2,1)} %bitcast.55), calls=%async_computation.3 | async-start | bytes 2883584 | tf_op jit(solution)/shard_map/all_to_all | solution.py:82
  103.0 48.7 %all-to-all-start.1 = ((bf16[512,4,352]{0,2,1:T(8,128)(2,1)}), bf16[512,4,352]{0,2,1:T(8,128)(2,1)S(1)}, u32[]{:S(2)}, u32[]{:S(2)}) async-start(bf16[512,4,352]{0,2,1:T(8,128)(2,1)} %bitcast.54), calls=%async_computation.1 | async-start | bytes 2883584 | tf_op jit(solution)/shard_map/all_to_all | solution.py:80
  151.7 38.8 %all-to-all-start.2 = ((bf16[512,4,352]{0,2,1:T(8,128)(2,1)}), bf16[512,4,352]{0,2,1:T(8,128)(2,1)}, u32[]{:S(2)}, u32[]{:S(2)}) async-start(bf16[512,4,352]{0,2,1:T(8,128)(2,1)} %bitcast.53), calls=%async_computation.2 | async-start | bytes 2883584 | tf_op jit(solution)/shard_map/all_to_all | solution.py:81
  156.0 123.4 %reduce-scatter.2.cloned.1.call-start = ((), (), s32[]{:S(2)}) async-start(), calls=%async_computation.7 | async-start | bytes 4456448 | tf_op jit(solution)/shard_map/reduce_scatter | solution.py:88
  158.7 34.5 %copy-start.2 = (bf16[4,44,8,512]{3,2,0,1:T(8,128)(2,1)S(1)}, bf16[4,44,8,512]{3,2,0,1:T(8,128)(2,1)}, u32[]{:S(2)}) copy-start(bf16[4,44,8,512]{3,2,0,1:T(8,128)(2,1)} %copy.40) | copy-start | bytes 4325380
  193.2 5.1 %copy-start.1 = (bf16[4,44,8,512]{3,2,0,1:T(8,128)(2,1)S(1)}, bf16[4,44,8,512]{3,2,0,1:T(8,128)(2,1)}, u32[]{:S(2)}) copy-start(bf16[4,44,8,512]{3,2,0,1:T(8,128)(2,1)} %copy.42) | copy-start | bytes 4325380
Sparse Core Ops, SparseCore 0:
  9.4 32.6 all-gather.2
  57.1 78.3 all-gather.4
  207.5 71.8 reduce-scatter.1

commit v2 on v1

--- a/solution.py
+++ b/solution.py
@@ -1,8 +1,11 @@
+import functools
 import math
 
 import jax
 import jax.numpy as jnp
 from jax import lax
+from jax.experimental import pallas as pl
+from jax.experimental.pallas import tpu as pltpu
 from jax.sharding import PartitionSpec as P
 
 HEAD_DIM = 64
@@ -91,9 +94,418 @@
     return (resid + back).astype(jnp.bfloat16)
 
 
+MESH = pl.DeviceIdType.MESH
+F32 = jnp.float32
+BF16 = jnp.bfloat16
+
+
+def layer_kernel(
+    dims, resid_ref, q_ref, k_ref, v_ref, gate_ref, gate_t_ref, gain_ref, w_out_ref, w_gate_ref,
+    w_up_ref, w_down_ref, out_ref, kbuf, vbuf, top, tot, acc, att, heads, w_out, resid, nall, wg,
+    wu, wd, part, crecv, csend, keep, xrecv, zsend, zrecv, loc_sem, kv_send, kv_recv, wz_send,
+    wz_recv, wy_send, wy_recv, h_send, h_recv, az_send, az_recv, ax_send, ax_recv, ac_send,
+    ac_recv, rc_send, rc_recv, rx_send, rx_recv, rz_send, rz_recv,
+):
+    ns, nt, chunk = dims
+    g, s, t = lax.axis_index("grp"), lax.axis_index("sp"), lax.axis_index("tp")
+    rows, width = resid_ref.shape
+    tok, att_w = q_ref.shape
+    depth, units = w_gate_ref.shape
+    nheads = att_w // HEAD_DIM
+    half_depth, half_chunk = depth // 2, chunk // 2
+    x, c = t // 2, t % 2
+    tx = (t + 2) % 4
+    tc = t + 1 - 2 * c
+    scale = HEAD_DIM ** (-0.5)
+
+    def start_of(i):
+        return pl.multiple_of(jnp.minimum(i * chunk, units - chunk), 128)
+
+    def remote(src, dst, send, recv, **where):
+        return pltpu.make_async_remote_copy(
+            src_ref=src, dst_ref=dst, send_sem=send, recv_sem=recv, device_id=where,
+            device_id_type=MESH,
+        )
+
+    def landing(mat, src, half):
+        if mat < 2:
+            return (wg, wu)[mat].at[pl.ds(pl.multiple_of(src * depth + half * half_depth, half_depth), half_depth)]
+        return wd.at[pl.ds(pl.multiple_of(half * half_chunk, half_chunk), half_chunk), pl.ds(pl.multiple_of(src * depth, depth), depth)]
+
+    def weight_out(mat, dst):
+        if mat < 2:
+            src = (w_gate_ref, w_up_ref)[mat].at[pl.ds(pl.multiple_of(g * half_depth, half_depth), half_depth), pl.ds(start_of(dst), chunk)]
+        else:
+            src = w_down_ref.at[pl.ds(pl.multiple_of(start_of(dst) + g * half_chunk, math.gcd(128, half_chunk)), half_chunk)]
+        return remote(src, landing(mat, s, g), wz_send.at[mat, dst], wz_recv.at[mat, s], sp=dst)
+
+    def weight_in(mat, src):
+        block = landing(mat, src, g)
+        return remote(block, block, wz_send.at[mat, src], wz_recv.at[mat, src], sp=src)
+
+    def weight_pass(mat, src, half):
+        block = landing(mat, src, half)
+        return remote(block, block, wy_send.at[mat, src], wy_recv.at[mat, src], grp=1 - g)
+
+    def each(low, high, body):
+        lax.fori_loop(low, high, lambda i, z: (body(i), z)[1], 0)
+
+    def others(body):
+        each(0, s, body)
+        each(s + 1, ns, body)
+
+    barrier = pltpu.get_barrier_semaphore()
+    others(lambda i: pl.semaphore_signal(barrier, inc=1, device_id={"sp": i}, device_id_type=MESH))
+    pl.semaphore_signal(barrier, inc=1, device_id={"grp": 1 - g}, device_id_type=MESH)
+    for j in range(1, nt):
+        pl.semaphore_signal(barrier, inc=1, device_id={"tp": (t + j) % nt}, device_id_type=MESH)
+    pl.semaphore_wait(barrier, ns + nt - 1)
+
+    def kv_out(i, kk, vv):
+        return (
+            remote(kk, kbuf.at[i], kv_send.at[0, i], kv_recv.at[0, i], sp=s + 1),
+            remote(vv, vbuf.at[i], kv_send.at[1, i], kv_recv.at[1, i], sp=s + 1),
+        )
+
+    def kv_in(i):
+        return (
+            remote(kbuf.at[i], kbuf.at[i], kv_send.at[0, i], kv_recv.at[0, i], sp=s - 1),
+            remote(vbuf.at[i], vbuf.at[i], kv_send.at[1, i], kv_recv.at[1, i], sp=s - 1),
+        )
+
+    @pl.when(s + 1 < ns)
+    def _():
+        for copy in kv_out(0, k_ref, v_ref):
+            copy.start()
+
+    def locals_():
+        own = pl.ds(pl.multiple_of(s * depth, depth), depth)
+        return (
+            pltpu.make_async_copy(w_out_ref, w_out, loc_sem.at[0]),
+            pltpu.make_async_copy(w_gate_ref.at[:, pl.ds(start_of(s), chunk)], wg.at[own], loc_sem.at[1]),
+            pltpu.make_async_copy(w_up_ref.at[:, pl.ds(start_of(s), chunk)], wu.at[own], loc_sem.at[2]),
+            pltpu.make_async_copy(w_down_ref.at[pl.ds(start_of(s), chunk)], wd.at[:, own], loc_sem.at[3]),
+        )
+
+    for copy in locals_():
+        copy.start()
+    for mat in range(3):
+        each(0, s, lambda i, mat=mat: weight_out(mat, s - 1 - i).start())
+
+    def start_up():
+        for mat in range(3):
+            each(s + 1, ns, lambda i, mat=mat: weight_out(mat, i).start())
+
+    pl.when(s == 0)(start_up)
+
+    gate_own = gate_ref[pl.ds(pl.multiple_of(s * tok, tok), tok), :]
+
+    def attend(src, kk, vv, first):
+        for h in range(nheads):
+            lanes = slice(h * HEAD_DIM, (h + 1) * HEAD_DIM)
+            scores = lax.dot_general(
+                q_ref[:, lanes], kk[:, lanes], (((1,), (1,)), ((), ())), preferred_element_type=F32
+            )
+            key_gate = gate_t_ref[h : h + 1, pl.ds(pl.multiple_of(src * tok, tok), tok)]
+            scores = scores * scale + gate_own[:, h : h + 1] - key_gate
+            if first:
+                row = lax.broadcasted_iota(jnp.int32, (tok, tok), 0)
+                col = lax.broadcasted_iota(jnp.int32, (tok, tok), 1)
+                scores = jnp.where(col <= row, scores, -1e30)
+                new = jnp.max(scores, axis=-1, keepdims=True)
+                w = jnp.where(col <= row, jnp.exp(scores - new), 0.0)
+                tot[h] = jnp.sum(w, axis=-1, keepdims=True)
+                acc[h] = jnp.dot(w.astype(BF16), vv[:, lanes], preferred_element_type=F32)
+            else:
+                old = top[h]
+                new = jnp.maximum(old, jnp.max(scores, axis=-1, keepdims=True))
+                w = jnp.exp(scores - new)
+                shrink = jnp.exp(old - new)
+                tot[h] = tot[h] * shrink + jnp.sum(w, axis=-1, keepdims=True)
+                acc[h] = acc[h] * shrink + jnp.dot(
+                    w.astype(BF16), vv[:, lanes], preferred_element_type=F32
+                )
+            top[h] = new
+
+    attend(s, k_ref, v_ref, True)
+
+    def earlier(i):
+        for copy in kv_in(i - 1):
+            copy.wait_recv()
+
+        @pl.when(s + 1 < ns)
+        def _():
+            for copy in kv_out(i, kbuf.at[i - 1], vbuf.at[i - 1]):
+                copy.start()
+
+        pl.when(i == s)(start_up)
+        attend(s - i, kbuf.at[i - 1], vbuf.at[i - 1], False)
+
+    each(1, s + 1, earlier)
+
+    for h in range(nheads):
+        att[:, h * HEAD_DIM : (h + 1) * HEAD_DIM] = (acc[h] / tot[h]).astype(BF16)
+
+    def head_copy(j):
+        dst = (t + j) % nt
+        return remote(
+            att.at[pl.ds(pl.multiple_of(dst * rows, rows), rows)], heads.at[j - 1],
+            h_send.at[j - 1], h_recv.at[j - 1], tp=dst,
+        )
+
+    for j in range(1, nt):
+        head_copy(j).start()
+
+    def pass_on(mat, src):
+        weight_in(mat, src).wait_recv()
+        weight_pass(mat, src, g).start()
+
+    copies = locals_()
+    copies[0].wait()
+    resid[...] = resid_ref[...].astype(F32) + jnp.dot(
+        att[pl.ds(pl.multiple_of(t * rows, rows), rows), :],
+        w_out[pl.ds(pl.multiple_of(t * att_w, att_w), att_w), :], preferred_element_type=F32,
+    )
+    each(s + 1, ns, lambda i: pass_on(0, i))
+
+    def mix(j):
+        head_copy(j).wait_recv()
+        src = (t + nt - j) % nt
+        resid[...] += jnp.dot(
+            heads[j - 1], w_out[pl.ds(pl.multiple_of(src * att_w, att_w), att_w), :],
+            preferred_element_type=F32,
+        )
+
+    each(1, nt, mix)
+    full = resid[...]
+    normed = full * lax.rsqrt(jnp.mean(full * full, axis=-1, keepdims=True) + 1e-06)
+    nall[s, t] = (normed * gain_ref[...]).astype(BF16)
+
+    def row_z(side, src, to):
+        block = nall.at[src, t]
+        return remote(block, block, az_send.at[side, src], az_recv.at[side, src], sp=to)
+
+    def row_x(src, who):
+        block = nall.at[src, who]
+        return remote(block, block, ax_send.at[src], ax_recv.at[src], tp=tx)
+
+    def row_c(kind, src, who):
+        block = nall.at[src, who]
+        return remote(block, block, ac_send.at[kind, src], ac_recv.at[kind, src], tp=tc)
+
+    def spread(src):
+        row_x(src, t).start()
+        row_c(0, src, t).start()
+
+    def relay(src):
+        row_x(src, tx).wait_recv()
+        row_c(1, src, tx).start()
+
+    pl.when(s + 1 < ns)(lambda: row_z(0, s, s + 1).start())
+    pl.when(s > 0)(lambda: row_z(1, s, s - 1).start())
+    spread(s)
+    each(s + 1, ns, lambda i: pass_on(1, i))
+    each(0, s, lambda i: pass_on(0, s - 1 - i))
+    relay(s)
+    each(s + 1, ns, lambda i: pass_on(2, i))
+    each(0, s, lambda i: pass_on(1, s - 1 - i))
+    each(0, s, lambda i: pass_on(2, s - 1 - i))
+
+    def gather(d):
+        @pl.when(s >= d)
+        def _():
+            row_z(0, s - d, s - 1).wait_recv()
+            pl.when(s + 1 < ns)(lambda: row_z(0, s - d, s + 1).start())
+            spread(s - d)
+
+        @pl.when(s + d < ns)
+        def _():
+            row_z(1, s + d, s + 1).wait_recv()
+            pl.when(s > 0)(lambda: row_z(1, s + d, s - 1).start())
+            spread(s + d)
+
+        @pl.when(d > 1)
+        def _():
+            pl.when(s >= d - 1)(lambda: relay(s - d + 1))
+            pl.when(s + d - 1 < ns)(lambda: relay(s + d - 1))
+
+    each(1, ns, gather)
+    pl.when(s >= ns - 1)(lambda: relay(s - ns + 1))
+    pl.when(s + ns - 1 < ns)(lambda: relay(s + ns - 1))
+
+    for copy in copies[1:]:
+        copy.wait()
+    for mat in range(3):
+        others(lambda i, mat=mat: weight_pass(mat, i, 1 - g).wait_recv())
+
+    def rows_in(src):
+        row_c(0, src, tc).wait_recv()
+        row_c(1, src, (tc + 2) % 4).wait_recv()
+
+    each(0, ns, rows_in)
+
+    fresh = lax.broadcasted_iota(jnp.int32, (tok, chunk), 1) + start_of(s) >= s * chunk
+    piece = math.gcd(width, 512)
+
+    def sum_c(d):
+        return remote(part.at[d, :, 1 - c], crecv.at[d], rc_send.at[d], rc_recv.at[d], tp=tc)
+
+    def sum_x(d):
+        return remote(csend.at[d], xrecv.at[d], rx_send.at[d], rx_recv.at[d], tp=tx)
+
+    def sum_z(d):
+        return remote(zsend.at[d], zrecv.at[d], rz_send.at[d], rz_recv.at[d], sp=(s + 1 + d) % ns)
+
+    def stage_x(d):
+        sum_c(d).wait_recv()
+        csend[d] = (part[d, 1 - x, c].astype(F32) + crecv[d, 1 - x].astype(F32)).astype(BF16)
+        sum_x(d).start()
+        keep[d] = part[d, x, c].astype(F32) + crecv[d, x].astype(F32)
+
+    def stage_z(d):
+        sum_x(d).wait_recv()
+        zsend[d] = (keep[d] + xrecv[d].astype(F32)).astype(BF16)
+        sum_z(d).start()
+
+    def feed(d):
+        dst = (s + 1 + d) % ns
+        a = nall[dst].reshape(tok, width)
+        gate = jnp.dot(a, wg[...], preferred_element_type=F32)
+        up = jnp.dot(a, wu[...], preferred_element_type=F32)
+        hidden = jnp.where(fresh, gate / (1.0 + jnp.exp(-gate)) * up, 0.0).astype(BF16)
+
+        def down(p):
+            cols = pl.ds(pl.multiple_of(p * piece, piece), piece)
+            y = jnp.dot(hidden, wd[:, cols], preferred_element_type=F32).astype(BF16)
+            part[d, :, :, :, cols] = y.reshape(2, 2, rows, piece)
+
+        each(0, width // piece, down)
+        sum_c(d).start()
+        pl.when(d >= 1)(lambda: stage_x(d - 1))
+        pl.when(d >= 2)(lambda: stage_z(d - 2))
+
+    each(0, ns, feed)
+    stage_x(ns - 1)
+    stage_z(ns - 2)
+    sum_x(ns - 1).wait_recv()
+    resid[...] += keep[ns - 1] + xrecv[ns - 1].astype(F32)
+
+    def last(d):
+        sum_z(d).wait_recv()
+        resid[...] += zrecv[d].astype(F32)
+
+    each(0, ns - 1, last)
+    out_ref[...] = resid[...].astype(BF16)
+
+    @pl.when(s + 1 < ns)
+    def _():
+        def sent(i):
+            for copy in kv_out(i, kbuf.at[0], vbuf.at[0]):
+                copy.wait_send()
+
+        each(0, s + 1, sent)
+        each(0, s + 1, lambda i: row_z(0, i, s + 1).wait_send())
+
+    pl.when(s > 0)(lambda: each(s, ns, lambda i: row_z(1, i, s - 1).wait_send()))
+    for mat in range(3):
+        others(lambda i, mat=mat: weight_out(mat, i).wait_send())
+        others(lambda i, mat=mat: weight_pass(mat, i, g).wait_send())
+    for j in range(1, nt):
+        head_copy(j).wait_send()
+
+    def spread_done(i):
+        row_x(i, t).wait_send()
+        row_c(0, i, t).wait_send()
+        row_c(1, i, tx).wait_send()
+        sum_c(i).wait_send()
+        sum_x(i).wait_send()
+
+    each(0, ns, spread_done)
+    each(0, ns - 1, lambda d: sum_z(d).wait_send())
+
+
+def fused(ns, nt, chunk, resid_in, queries, keys, values, cum_gate, w_out, norm_gain, w_gate, w_up, w_down):
+    rows, width = resid_in.shape
+    tok, att_w = queries.shape
+    depth, units = w_gate.shape
+    nheads = att_w // HEAD_DIM
+    vm = pl.BlockSpec(memory_space=pltpu.VMEM)
+    hbm = pl.BlockSpec(memory_space=pltpu.HBM)
+    dma = pltpu.SemaphoreType.DMA
+    return pl.pallas_call(
+        functools.partial(layer_kernel, (ns, nt, chunk)),
+        out_shape=jax.ShapeDtypeStruct((rows, width), BF16),
+        in_specs=[vm] * 7 + [hbm] * 4,
+        out_specs=vm,
+        scratch_shapes=[
+            pltpu.VMEM((ns - 1, tok, att_w), BF16),
+            pltpu.VMEM((ns - 1, tok, att_w), BF16),
+            pltpu.VMEM((nheads, tok, 1), F32),
+            pltpu.VMEM((nheads, tok, 1), F32),
+            pltpu.VMEM((nheads, tok, HEAD_DIM), F32),
+            pltpu.VMEM((tok, att_w), BF16),
+            pltpu.VMEM((nt - 1, rows, att_w), BF16),
+            pltpu.VMEM(w_out.shape, BF16),
+            pltpu.VMEM((rows, width), F32),
+            pltpu.VMEM((ns, nt, rows, width), BF16),
+            pltpu.VMEM((width, chunk), BF16),
+            pltpu.VMEM((width, chunk), BF16),
+            pltpu.VMEM((chunk, width), BF16),
+            pltpu.VMEM((ns, 2, 2, rows, width), BF16),
+            pltpu.VMEM((ns, 2, rows, width), BF16),
+            pltpu.VMEM((ns, rows, width), BF16),
+            pltpu.VMEM((ns, rows, width), F32),
+            pltpu.VMEM((ns, rows, width), BF16),
+            pltpu.VMEM((ns, rows, width), BF16),
+            pltpu.VMEM((ns, rows, width), BF16),
+            dma((4,)),
+            dma((2, ns)), dma((2, ns)),
+            dma((3, ns)), dma((3, ns)),
+            dma((3, ns)), dma((3, ns)),
+            dma((nt - 1,)), dma((nt - 1,)),
+            dma((2, ns)), dma((2, ns)),
+            dma((ns,)), dma((ns,)),
+            dma((2, ns)), dma((2, ns)),
+            dma((ns,)), dma((ns,)),
+            dma((ns,)), dma((ns,)),
+            dma((ns,)), dma((ns,)),
+        ],
+        compiler_params=pltpu.CompilerParams(
+            collective_id=0, has_side_effects=True, vmem_limit_bytes=60 * 2**20
+        ),
+        name="layer",
+    )(
+        resid_in, queries, keys, values, cum_gate, cum_gate.T, norm_gain[None, :], w_out, w_gate,
+        w_up, w_down,
+    )
+
+
+def pick(mesh):
+    ng, ns, nt = (mesh.shape[a] for a in ("grp", "sp", "tp"))
+
+    def step(*args):
+        resid_in, queries, cum_gate, w_gate = args[0], args[1], args[4], args[7]
+        rows, width = resid_in.shape
+        depth, units = w_gate.shape
+        chunk = -(-units // (128 * ns)) * 128
+        need = 2 * ns * nt * rows * width * 4 + 6 * width * chunk + 2 * args[5].size
+        fits = (
+            ng == 2 and nt == 4 and ns > 1 and units % 128 == 0 and (ns - 1) * chunk < units
+            and depth % 256 == 0 and width == ns * depth and rows % 16 == 0
+            and queries.shape[0] == rows * nt and queries.shape[0] % 128 == 0
+            and cum_gate.shape[0] == ns * nt * rows and queries.shape[1] % 128 == 0
+            and need < 40 * 2**20
+        )
+        if fits:
+            return fused(ns, nt, chunk, *args)
+        return on_device(*args)
+
+    return step
+
+
 def solution(mesh):
     return jax.shard_map(
-        on_device,
+        pick(mesh),
         mesh=mesh,
         in_specs=(
             P(("grp", "sp", "tp"), None),

time: 288 us -> 139 us (0.48)
  the two profiles are of different devices: /device:TPU:0 before, /device:TPU:9 now
where the time goes in v2:
time: 139 us
  Pallas kernels  136 us (98%)
  local copies, waits for them, and re-layouts  3.4 us (2%)
    pallas_call x1, Pallas kernels, fused(): pl.pallas_call(functools.partial(layer_kernel, (ns, nt, chunk)), out_shap...  136 us
    unnamed x2, local copies, waits for them, and re-layouts  3.4 us

profile of v2, /device:TPU:9, one launch (start us, length us, event | category | flops | bytes accessed | tf_op | source)
XLA Modules:
  0.0 139.1 jit_solution(4012710605290026008)
XLA Ops:
  0.0 1.7 %copy.11.gate_ref = f32[1024,4]{1,0:T(8,128)} copy(f32[1024,4]{0,1:T(4,128)} %param.14) | data formatting | bytes 32768 | tf_op args[4]
  1.7 135.7 %layer.1 = bf16[64,2048]{1,0:T(8,128)(2,1)} custom-call(bf16[64,2048]{1,0:T(8,128)(2,1)} %resid_ref.1, bf16[256,256]{1,0:T(8,128)(2,1)} %q_ref.1, bf16[256,256]{1,0:T(8,128)(2,1)} %k_ref.1, bf16[256,256]{1,0:T(8,128)(2,1)} %v_ref.1, f32[1024,4]{1,0:T(8,128)} %copy.11.gate_ref, f32[4,1024]{1,0:T(4,128)} %bitcast.2, f32[1,2048]{1,0:T(1,128)} %bitcast.3, ...), custom_call_target="tpu_custom_call" | custom-call | tf_op jit(solution)/shard_map/layer/pallas_call | solution.py:435
  137.5 1.7 %copy.13 = bf16[64,2048]{1,0:T(8,128)(2,1)} copy(bf16[64,2048]{1,0:T(8,128)(2,1)} %layer.1) | data formatting | bytes 524288

commit v3 on v2

--- a/solution.py
+++ b/solution.py
@@ -104,7 +104,7 @@
     w_up_ref, w_down_ref, out_ref, kbuf, vbuf, top, tot, acc, att, heads, w_out, resid, nall, wg,
     wu, wd, part, crecv, csend, keep, xrecv, zsend, zrecv, loc_sem, kv_send, kv_recv, wz_send,
     wz_recv, wy_send, wy_recv, h_send, h_recv, az_send, az_recv, ax_send, ax_recv, ac_send,
-    ac_recv, rc_send, rc_recv, rx_send, rx_recv, rz_send, rz_recv,
+    ac_recv, rc_send, rc_recv, rx_send, rx_recv, rz_send, rz_recv, go,
 ):
     ns, nt, chunk = dims
     g, s, t = lax.axis_index("grp"), lax.axis_index("sp"), lax.axis_index("tp")
@@ -112,7 +112,8 @@
     tok, att_w = q_ref.shape
     depth, units = w_gate_ref.shape
     nheads = att_w // HEAD_DIM
-    half_depth, half_chunk = depth // 2, chunk // 2
+    half_depth = depth // 2
+    dup = ns * chunk - units
     x, c = t // 2, t % 2
     tx = (t + 2) % 4
     tc = t + 1 - 2 * c
@@ -127,25 +128,48 @@
             device_id_type=MESH,
         )
 
-    def landing(mat, src, half):
+    def xor(a, b):
+        hi, lo, bh, bl = a // 2, a % 2, b // 2, b % 2
+        return 2 * (hi + bh - 2 * hi * bh) + lo + bl - 2 * lo * bl
+
+    def landing(mat, src, half, skip):
         if mat < 2:
-            return (wg, wu)[mat].at[pl.ds(pl.multiple_of(src * depth + half * half_depth, half_depth), half_depth)]
-        return wd.at[pl.ds(pl.multiple_of(half * half_chunk, half_chunk), half_chunk), pl.ds(pl.multiple_of(src * depth, depth), depth)]
-
-    def weight_out(mat, dst):
+            return (wg, wu)[mat].at[
+                pl.ds(pl.multiple_of(src * depth + half * half_depth, half_depth), half_depth),
+                pl.ds(skip, chunk - skip),
+            ]
+        size = (chunk - skip) // 2
+        return wd.at[
+            pl.ds(pl.multiple_of(skip + half * size, math.gcd(128, size)), size),
+            pl.ds(pl.multiple_of(src * depth, depth), depth),
+        ]
+
+    def weight_out(mat, dst, skip):
         if mat < 2:
-            src = (w_gate_ref, w_up_ref)[mat].at[pl.ds(pl.multiple_of(g * half_depth, half_depth), half_depth), pl.ds(start_of(dst), chunk)]
+            src = (w_gate_ref, w_up_ref)[mat].at[
+                pl.ds(pl.multiple_of(g * half_depth, half_depth), half_depth),
+                pl.ds(pl.multiple_of(start_of(dst) + skip, 128), chunk - skip),
+            ]
         else:
-            src = w_down_ref.at[pl.ds(pl.multiple_of(start_of(dst) + g * half_chunk, math.gcd(128, half_chunk)), half_chunk)]
-        return remote(src, landing(mat, s, g), wz_send.at[mat, dst], wz_recv.at[mat, s], sp=dst)
-
-    def weight_in(mat, src):
-        block = landing(mat, src, g)
+            size = (chunk - skip) // 2
+            src = w_down_ref.at[
+                pl.ds(pl.multiple_of(start_of(dst) + skip + g * size, math.gcd(128, size)), size)
+            ]
+        return remote(
+            src, landing(mat, s, g, skip), wz_send.at[mat, dst], wz_recv.at[mat, s], sp=dst
+        )
+
+    def weight_in(mat, src, skip):
+        block = landing(mat, src, g, skip)
         return remote(block, block, wz_send.at[mat, src], wz_recv.at[mat, src], sp=src)
 
-    def weight_pass(mat, src, half):
-        block = landing(mat, src, half)
+    def weight_pass(mat, src, half, skip):
+        block = landing(mat, src, half, skip)
         return remote(block, block, wy_send.at[mat, src], wy_recv.at[mat, src], grp=1 - g)
+
+    def sized(dst, body):
+        pl.when(dst < ns - 1)(lambda: body(0))
+        pl.when(dst == ns - 1)(lambda: body(dup))
 
     def each(low, high, body):
         lax.fori_loop(low, high, lambda i, z: (body(i), z)[1], 0)
@@ -189,14 +213,23 @@
 
     for copy in locals_():
         copy.start()
-    for mat in range(3):
-        each(0, s, lambda i, mat=mat: weight_out(mat, s - 1 - i).start())
-
-    def start_up():
-        for mat in range(3):
-            each(s + 1, ns, lambda i, mat=mat: weight_out(mat, i).start())
-
-    pl.when(s == 0)(start_up)
+    def send_weight(mat, dst):
+        sized(dst, lambda skip: weight_out(mat, dst, skip).start())
+
+    for mat in range(2):
+        each(0, s, lambda i, mat=mat: send_weight(mat, s - 1 - i))
+
+    if dup:
+
+        @pl.when(s == ns - 1)
+        def _():
+            for mat in range(2):
+                def clear(i, mat=mat):
+                    band = pl.ds(pl.multiple_of((i + (i >= s)) * depth, depth), depth)
+                    (wg, wu)[mat][band, :dup] = jnp.zeros((depth, dup), BF16)
+
+                each(0, ns - 1, clear)
+            wd[:dup, : (ns - 1) * depth] = jnp.zeros((dup, (ns - 1) * depth), BF16)
 
     gate_own = gate_ref[pl.ds(pl.multiple_of(s * tok, tok), tok), :]
 
@@ -238,7 +271,15 @@
             for copy in kv_out(i, kbuf.at[i - 1], vbuf.at[i - 1]):
                 copy.start()
 
-        pl.when(i == s)(start_up)
+        @pl.when((i == s) & (s == ns - 2))
+        def _():
+            each(
+                0, s,
+                lambda j: pl.semaphore_signal(
+                    go, inc=1, device_id={"sp": j}, device_id_type=MESH
+                ),
+            )
+
         attend(s - i, kbuf.at[i - 1], vbuf.at[i - 1], False)
 
     each(1, s + 1, earlier)
@@ -257,8 +298,11 @@
         head_copy(j).start()
 
     def pass_on(mat, src):
-        weight_in(mat, src).wait_recv()
-        weight_pass(mat, src, g).start()
+        def body(skip):
+            weight_in(mat, src, skip).wait_recv()
+            weight_pass(mat, src, g, skip).start()
+
+        sized(s, body)
 
     copies = locals_()
     copies[0].wait()
@@ -266,7 +310,6 @@
         att[pl.ds(pl.multiple_of(t * rows, rows), rows), :],
         w_out[pl.ds(pl.multiple_of(t * att_w, att_w), att_w), :], preferred_element_type=F32,
     )
-    each(s + 1, ns, lambda i: pass_on(0, i))
 
     def mix(j):
         head_copy(j).wait_recv()
@@ -281,9 +324,13 @@
     normed = full * lax.rsqrt(jnp.mean(full * full, axis=-1, keepdims=True) + 1e-06)
     nall[s, t] = (normed * gain_ref[...]).astype(BF16)
 
-    def row_z(side, src, to):
+    def row_z(src, to):
         block = nall.at[src, t]
-        return remote(block, block, az_send.at[side, src], az_recv.at[side, src], sp=to)
+        return remote(block, block, az_send.at[0, src], az_recv.at[src], sp=to)
+
+    def row_far(to):
+        block = nall.at[s, t]
+        return remote(block, block, az_send.at[1, s], az_recv.at[s], sp=to)
 
     def row_x(src, who):
         block = nall.at[src, who]
@@ -301,42 +348,44 @@
         row_x(src, tx).wait_recv()
         row_c(1, src, tx).start()
 
-    pl.when(s + 1 < ns)(lambda: row_z(0, s, s + 1).start())
-    pl.when(s > 0)(lambda: row_z(1, s, s - 1).start())
+    near, far, cross = xor(s, 1), xor(s, 2), xor(s, 3)
+    pl.when(s < ns - 2)(lambda: pl.semaphore_wait(go, 1))
+    row_far(far).start()
+    row_z(s, near).start()
+    for mat in range(2):
+        each(s + 1, ns, lambda i, mat=mat: send_weight(mat, i))
+    each(0, s, lambda i: send_weight(2, s - 1 - i))
+    each(s + 1, ns, lambda i: send_weight(2, i))
     spread(s)
-    each(s + 1, ns, lambda i: pass_on(1, i))
-    each(0, s, lambda i: pass_on(0, s - 1 - i))
+
+    def take_far():
+        row_z(far, far).wait_recv()
+        row_z(far, near).start()
+        spread(far)
+
+    def take(src):
+        row_z(src, near).wait_recv()
+        spread(src)
+
+    for mat in range(2):
+        each(s + 1, ns, lambda i, mat=mat: pass_on(mat, i))
     relay(s)
+    pl.when(s >= 2)(take_far)
+    for mat in range(2):
+        each(0, s, lambda i, mat=mat: pass_on(mat, s - 1 - i))
+    pl.when(s < 2)(take_far)
+    take(near)
+    relay(far)
+    take(cross)
+    relay(near)
     each(s + 1, ns, lambda i: pass_on(2, i))
-    each(0, s, lambda i: pass_on(1, s - 1 - i))
     each(0, s, lambda i: pass_on(2, s - 1 - i))
-
-    def gather(d):
-        @pl.when(s >= d)
-        def _():
-            row_z(0, s - d, s - 1).wait_recv()
-            pl.when(s + 1 < ns)(lambda: row_z(0, s - d, s + 1).start())
-            spread(s - d)
-
-        @pl.when(s + d < ns)
-        def _():
-            row_z(1, s + d, s + 1).wait_recv()
-            pl.when(s > 0)(lambda: row_z(1, s + d, s - 1).start())
-            spread(s + d)
-
-        @pl.when(d > 1)
-        def _():
-            pl.when(s >= d - 1)(lambda: relay(s - d + 1))
-            pl.when(s + d - 1 < ns)(lambda: relay(s + d - 1))
-
-    each(1, ns, gather)
-    pl.when(s >= ns - 1)(lambda: relay(s - ns + 1))
-    pl.when(s + ns - 1 < ns)(lambda: relay(s + ns - 1))
+    relay(cross)
 
     for copy in copies[1:]:
         copy.wait()
     for mat in range(3):
-        others(lambda i, mat=mat: weight_pass(mat, i, 1 - g).wait_recv())
+        others(lambda i, mat=mat: sized(s, lambda skip: weight_pass(mat, i, 1 - g, skip).wait_recv()))
 
     def rows_in(src):
         row_c(0, src, tc).wait_recv()
@@ -354,7 +403,7 @@
         return remote(csend.at[d], xrecv.at[d], rx_send.at[d], rx_recv.at[d], tp=tx)
 
     def sum_z(d):
-        return remote(zsend.at[d], zrecv.at[d], rz_send.at[d], rz_recv.at[d], sp=(s + 1 + d) % ns)
+        return remote(zsend.at[d], zrecv.at[d], rz_send.at[d], rz_recv.at[d], sp=xor(s, 1 + d % 2))
 
     def stage_x(d):
         sum_c(d).wait_recv()
@@ -364,11 +413,18 @@
 
     def stage_z(d):
         sum_x(d).wait_recv()
-        zsend[d] = (keep[d] + xrecv[d].astype(F32)).astype(BF16)
+        keep[d] = keep[d] + xrecv[d].astype(F32)
+
+        @pl.when(d == 1)
+        def _():
+            sum_z(0).wait_recv()
+            keep[1] = keep[1] + zrecv[0].astype(F32)
+
+        zsend[d] = keep[d].astype(BF16)
         sum_z(d).start()
 
     def feed(d):
-        dst = (s + 1 + d) % ns
+        dst = xor(s, 3 - d)
         a = nall[dst].reshape(tok, width)
         gate = jnp.dot(a, wg[...], preferred_element_type=F32)
         up = jnp.dot(a, wu[...], preferred_element_type=F32)
@@ -390,11 +446,9 @@
     sum_x(ns - 1).wait_recv()
     resid[...] += keep[ns - 1] + xrecv[ns - 1].astype(F32)
 
-    def last(d):
+    for d in (1, 2):
         sum_z(d).wait_recv()
         resid[...] += zrecv[d].astype(F32)
-
-    each(0, ns - 1, last)
     out_ref[...] = resid[...].astype(BF16)
 
     @pl.when(s + 1 < ns)
@@ -404,12 +458,13 @@
                 copy.wait_send()
 
         each(0, s + 1, sent)
-        each(0, s + 1, lambda i: row_z(0, i, s + 1).wait_send())
-
-    pl.when(s > 0)(lambda: each(s, ns, lambda i: row_z(1, i, s - 1).wait_send()))
+
+    row_far(far).wait_send()
+    row_z(s, near).wait_send()
+    row_z(far, near).wait_send()
     for mat in range(3):
-        others(lambda i, mat=mat: weight_out(mat, i).wait_send())
-        others(lambda i, mat=mat: weight_pass(mat, i, g).wait_send())
+        others(lambda i, mat=mat: sized(i, lambda skip: weight_out(mat, i, skip).wait_send()))
+        others(lambda i, mat=mat: sized(s, lambda skip: weight_pass(mat, i, g, skip).wait_send()))
     for j in range(1, nt):
         head_copy(j).wait_send()
 
@@ -463,12 +518,13 @@
             dma((3, ns)), dma((3, ns)),
             dma((3, ns)), dma((3, ns)),
             dma((nt - 1,)), dma((nt - 1,)),
-            dma((2, ns)), dma((2, ns)),
+            dma((2, ns)), dma((ns,)),
             dma((ns,)), dma((ns,)),
             dma((2, ns)), dma((2, ns)),
             dma((ns,)), dma((ns,)),
             dma((ns,)), dma((ns,)),
             dma((ns,)), dma((ns,)),
+            pltpu.SemaphoreType.REGULAR,
         ],
         compiler_params=pltpu.CompilerParams(
             collective_id=0, has_side_effects=True, vmem_limit_bytes=60 * 2**20
@@ -490,8 +546,8 @@
         chunk = -(-units // (128 * ns)) * 128
         need = 2 * ns * nt * rows * width * 4 + 6 * width * chunk + 2 * args[5].size
         fits = (
-            ng == 2 and nt == 4 and ns > 1 and units % 128 == 0 and (ns - 1) * chunk < units
-            and depth % 256 == 0 and width == ns * depth and rows % 16 == 0
+            ng == 2 and nt == 4 and ns == 4 and units % 128 == 0 and (ns - 1) * chunk < units
+            and depth % 256 == 0 and (chunk - ns * chunk + units) % 32 == 0 and width == ns * depth and rows % 16 == 0
             and queries.shape[0] == rows * nt and queries.shape[0] % 128 == 0
             and cum_gate.shape[0] == ns * nt * rows and queries.shape[1] % 128 == 0
             and need < 40 * 2**20

time: 139 us -> 125 us (0.90)
  the two profiles are of different devices: /device:TPU:9 before, /device:TPU:0 now
where the time goes in v3:
time: 125 us; the launch traced here: 124 us
  Pallas kernels  121 us (97%)
  local copies, waits for them, and re-layouts  3.4 us (3%)
    pallas_call x1, Pallas kernels, fused(): pl.pallas_call(functools.partial(layer_kernel, (ns, nt, chunk)), out_shap...  121 us
    unnamed x2, local copies, waits for them, and re-layouts  3.4 us

profile of v3, /device:TPU:0, one launch (start us, length us, event | category | flops | bytes accessed | tf_op | source)
XLA Modules:
  0.0 124.3 jit_solution(16931129831305051800)
XLA Ops:
  0.0 1.7 %copy.11.gate_ref = f32[1024,4]{1,0:T(8,128)} copy(f32[1024,4]{0,1:T(4,128)} %param.14) | data formatting | bytes 32768 | tf_op args[4]
  1.7 120.9 %layer.1 = bf16[64,2048]{1,0:T(8,128)(2,1)} custom-call(bf16[64,2048]{1,0:T(8,128)(2,1)} %resid_ref.1, bf16[256,256]{1,0:T(8,128)(2,1)} %q_ref.1, bf16[256,256]{1,0:T(8,128)(2,1)} %k_ref.1, bf16[256,256]{1,0:T(8,128)(2,1)} %v_ref.1, f32[1024,4]{1,0:T(8,128)} %copy.11.gate_ref, f32[4,1024]{1,0:T(4,128)} %bitcast.2, f32[1,2048]{1,0:T(1,128)} %bitcast.3, ...), custom_call_target="tpu_custom_call" | custom-call | tf_op jit(solution)/shard_map/layer/pallas_call | solution.py:490
  122.6 1.7 %copy.13 = bf16[64,2048]{1,0:T(8,128)(2,1)} copy(bf16[64,2048]{1,0:T(8,128)(2,1)} %layer.1) | data formatting | bytes 524288

commit v4 on v3

--- a/solution.py
+++ b/solution.py
@@ -100,9 +100,9 @@
 
 
 def layer_kernel(
-    dims, resid_ref, q_ref, k_ref, v_ref, gate_ref, gate_t_ref, gain_ref, w_out_ref, w_gate_ref,
+    dims, resid_ref, q_ref, k_ref, v_ref, gate_t_ref, gain_ref, w_out_ref, w_gate_ref,
     w_up_ref, w_down_ref, out_ref, kbuf, vbuf, top, tot, acc, att, heads, w_out, resid, nall, wg,
-    wu, wd, part, crecv, csend, keep, xrecv, zsend, zrecv, loc_sem, kv_send, kv_recv, wz_send,
+    wu, wd, hidden, part, crecv, csend, keep, xrecv, zsend, zrecv, loc_sem, kv_send, kv_recv, wz_send,
     wz_recv, wy_send, wy_recv, h_send, h_recv, az_send, az_recv, ax_send, ax_recv, ac_send,
     ac_recv, rc_send, rc_recv, rx_send, rx_recv, rz_send, rz_recv, go,
 ):
@@ -231,7 +231,7 @@
                 each(0, ns - 1, clear)
             wd[:dup, : (ns - 1) * depth] = jnp.zeros((dup, (ns - 1) * depth), BF16)
 
-    gate_own = gate_ref[pl.ds(pl.multiple_of(s * tok, tok), tok), :]
+    gate_own = gate_t_ref[:, pl.ds(pl.multiple_of(s * tok, tok), tok)].T
 
     def attend(src, kk, vv, first):
         for h in range(nheads):
@@ -378,23 +378,33 @@
     relay(far)
     take(cross)
     relay(near)
+
+    for copy in copies[1:]:
+        copy.wait()
+
+    def twin_in(mat):
+        others(lambda i: sized(s, lambda skip: weight_pass(mat, i, 1 - g, skip).wait_recv()))
+
+    twin_in(0)
+    twin_in(1)
+    fresh = lax.broadcasted_iota(jnp.int32, (tok, chunk), 1) + start_of(s) >= s * chunk
+    half = width // 2
+    piece = math.gcd(half, 512)
+
+    def hide(src):
+        row_c(0, src, tc).wait_recv()
+        row_c(1, src, (tc + 2) % 4).wait_recv()
+        a = nall[src].reshape(tok, width)
+        gate = jnp.dot(a, wg[...], preferred_element_type=F32)
+        up = jnp.dot(a, wu[...], preferred_element_type=F32)
+        hidden[src] = jnp.where(fresh, gate / (1.0 + jnp.exp(-gate)) * up, 0.0).astype(BF16)
+
+    each(0, ns - 1, lambda k: hide(xor(s, k)))
     each(s + 1, ns, lambda i: pass_on(2, i))
     each(0, s, lambda i: pass_on(2, s - 1 - i))
     relay(cross)
-
-    for copy in copies[1:]:
-        copy.wait()
-    for mat in range(3):
-        others(lambda i, mat=mat: sized(s, lambda skip: weight_pass(mat, i, 1 - g, skip).wait_recv()))
-
-    def rows_in(src):
-        row_c(0, src, tc).wait_recv()
-        row_c(1, src, (tc + 2) % 4).wait_recv()
-
-    each(0, ns, rows_in)
-
-    fresh = lax.broadcasted_iota(jnp.int32, (tok, chunk), 1) + start_of(s) >= s * chunk
-    piece = math.gcd(width, 512)
+    hide(cross)
+    twin_in(2)
 
     def sum_c(d):
         return remote(part.at[d, :, 1 - c], crecv.at[d], rc_send.at[d], rc_recv.at[d], tp=tc)
@@ -403,7 +413,7 @@
         return remote(csend.at[d], xrecv.at[d], rx_send.at[d], rx_recv.at[d], tp=tx)
 
     def sum_z(d):
-        return remote(zsend.at[d], zrecv.at[d], rz_send.at[d], rz_recv.at[d], sp=xor(s, 1 + d % 2))
+        return remote(zsend.at[d], zrecv.at[d], rz_send.at[d], rz_recv.at[d], sp=xor(s, 1 + d // 2 % 2))
 
     def stage_x(d):
         sum_c(d).wait_recv()
@@ -415,40 +425,39 @@
         sum_x(d).wait_recv()
         keep[d] = keep[d] + xrecv[d].astype(F32)
 
-        @pl.when(d == 1)
+        @pl.when((d == 2) | (d == 3))
         def _():
-            sum_z(0).wait_recv()
-            keep[1] = keep[1] + zrecv[0].astype(F32)
+            sum_z(d - 2).wait_recv()
+            keep[d] = keep[d] + zrecv[d - 2].astype(F32)
 
         zsend[d] = keep[d].astype(BF16)
         sum_z(d).start()
 
     def feed(d):
-        dst = xor(s, 3 - d)
-        a = nall[dst].reshape(tok, width)
-        gate = jnp.dot(a, wg[...], preferred_element_type=F32)
-        up = jnp.dot(a, wu[...], preferred_element_type=F32)
-        hidden = jnp.where(fresh, gate / (1.0 + jnp.exp(-gate)) * up, 0.0).astype(BF16)
+        src = hidden[xor(s, 3 - d // 2)]
 
         def down(p):
             cols = pl.ds(pl.multiple_of(p * piece, piece), piece)
-            y = jnp.dot(hidden, wd[:, cols], preferred_element_type=F32).astype(BF16)
+            from_ = pl.ds(pl.multiple_of(d % 2 * half + p * piece, piece), piece)
+            y = jnp.dot(src, wd[:, from_], preferred_element_type=F32).astype(BF16)
             part[d, :, :, :, cols] = y.reshape(2, 2, rows, piece)
 
-        each(0, width // piece, down)
+        each(0, half // piece, down)
         sum_c(d).start()
         pl.when(d >= 1)(lambda: stage_x(d - 1))
-        pl.when(d >= 2)(lambda: stage_z(d - 2))
-
-    each(0, ns, feed)
-    stage_x(ns - 1)
-    stage_z(ns - 2)
-    sum_x(ns - 1).wait_recv()
-    resid[...] += keep[ns - 1] + xrecv[ns - 1].astype(F32)
-
-    for d in (1, 2):
-        sum_z(d).wait_recv()
-        resid[...] += zrecv[d].astype(F32)
+        pl.when(d >= 3)(lambda: stage_z(d - 3))
+
+    each(0, 2 * ns, feed)
+    stage_x(2 * ns - 1)
+    stage_z(2 * ns - 3)
+    for d in (6, 7):
+        cols = slice((d - 6) * half, (d - 5) * half)
+        sum_x(d).wait_recv()
+        sum_z(d - 4).wait_recv()
+        sum_z(d - 2).wait_recv()
+        resid[:, cols] += (
+            keep[d] + xrecv[d].astype(F32) + zrecv[d - 4].astype(F32) + zrecv[d - 2].astype(F32)
+        )
     out_ref[...] = resid[...].astype(BF16)
 
     @pl.when(s + 1 < ns)
@@ -472,11 +481,15 @@
         row_x(i, t).wait_send()
         row_c(0, i, t).wait_send()
         row_c(1, i, tx).wait_send()
-        sum_c(i).wait_send()
-        sum_x(i).wait_send()
 
     each(0, ns, spread_done)
-    each(0, ns - 1, lambda d: sum_z(d).wait_send())
+
+    def sums_done(d):
+        sum_c(d).wait_send()
+        sum_x(d).wait_send()
+
+    each(0, 2 * ns, sums_done)
+    each(0, 2 * ns - 2, lambda d: sum_z(d).wait_send())
 
 
 def fused(ns, nt, chunk, resid_in, queries, keys, values, cum_gate, w_out, norm_gain, w_gate, w_up, w_down):
@@ -490,7 +503,7 @@
     return pl.pallas_call(
         functools.partial(layer_kernel, (ns, nt, chunk)),
         out_shape=jax.ShapeDtypeStruct((rows, width), BF16),
-        in_specs=[vm] * 7 + [hbm] * 4,
+        in_specs=[vm] * 6 + [hbm] * 4,
         out_specs=vm,
         scratch_shapes=[
             pltpu.VMEM((ns - 1, tok, att_w), BF16),
@@ -506,13 +519,14 @@
             pltpu.VMEM((width, chunk), BF16),
             pltpu.VMEM((width, chunk), BF16),
             pltpu.VMEM((chunk, width), BF16),
-            pltpu.VMEM((ns, 2, 2, rows, width), BF16),
-            pltpu.VMEM((ns, 2, rows, width), BF16),
-            pltpu.VMEM((ns, rows, width), BF16),
-            pltpu.VMEM((ns, rows, width), F32),
-            pltpu.VMEM((ns, rows, width), BF16),
-            pltpu.VMEM((ns, rows, width), BF16),
-            pltpu.VMEM((ns, rows, width), BF16),
+            pltpu.VMEM((ns, tok, chunk), BF16),
+            pltpu.VMEM((2 * ns, 2, 2, rows, width // 2), BF16),
+            pltpu.VMEM((2 * ns, 2, rows, width // 2), BF16),
+            pltpu.VMEM((2 * ns, rows, width // 2), BF16),
+            pltpu.VMEM((2 * ns, rows, width // 2), F32),
+            pltpu.VMEM((2 * ns, rows, width // 2), BF16),
+            pltpu.VMEM((2 * ns, rows, width // 2), BF16),
+            pltpu.VMEM((2 * ns, rows, width // 2), BF16),
             dma((4,)),
             dma((2, ns)), dma((2, ns)),
             dma((3, ns)), dma((3, ns)),
@@ -521,9 +535,9 @@
             dma((2, ns)), dma((ns,)),
             dma((ns,)), dma((ns,)),
             dma((2, ns)), dma((2, ns)),
-            dma((ns,)), dma((ns,)),
-            dma((ns,)), dma((ns,)),
-            dma((ns,)), dma((ns,)),
+            dma((2 * ns,)), dma((2 * ns,)),
+            dma((2 * ns,)), dma((2 * ns,)),
+            dma((2 * ns,)), dma((2 * ns,)),
             pltpu.SemaphoreType.REGULAR,
         ],
         compiler_params=pltpu.CompilerParams(
@@ -531,7 +545,7 @@
         ),
         name="layer",
     )(
-        resid_in, queries, keys, values, cum_gate, cum_gate.T, norm_gain[None, :], w_out, w_gate,
+        resid_in, queries, keys, values, cum_gate.T, norm_gain[None, :], w_out, w_gate,
         w_up, w_down,
     )
 
@@ -547,7 +561,7 @@
         need = 2 * ns * nt * rows * width * 4 + 6 * width * chunk + 2 * args[5].size
         fits = (
             ng == 2 and nt == 4 and ns == 4 and units % 128 == 0 and (ns - 1) * chunk < units
-            and depth % 256 == 0 and (chunk - ns * chunk + units) % 32 == 0 and width == ns * depth and rows % 16 == 0
+            and depth % 256 == 0 and width % 256 == 0 and (chunk - ns * chunk + units) % 32 == 0 and width == ns * depth and rows % 16 == 0
             and queries.shape[0] == rows * nt and queries.shape[0] % 128 == 0
             and cum_gate.shape[0] == ns * nt * rows and queries.shape[1] % 128 == 0
             and need < 40 * 2**20

time: 125 us -> 126 us (level)
  Pallas kernels: 121 us -> 124 us
  local copies, waits for them, and re-layouts: 3.4 us -> 1.67 us
    pallas_call x1, Pallas kernels: 121 us -> 124 us  [fused(): pl.pallas_call(functools.partial(layer_kernel, (ns, nt, chunk)), out_shap...]
    unnamed x2 -> x1, local copies, waits for them, and re-layouts: 3.4 us -> 1.67 us
where the time goes in v4:
time: 126 us
  Pallas kernels  124 us (98%)
  local copies, waits for them, and re-layouts  1.67 us (1%)
    pallas_call x1, Pallas kernels, fused(): pl.pallas_call(functools.partial(layer_kernel, (ns, nt, chunk)), out_shap...  124 us

profile of v4, /device:TPU:0, one launch (start us, length us, event | category | flops | bytes accessed | tf_op | source)
XLA Modules:
  0.0 125.5 jit_solution(17601040577878913193)
XLA Ops:
  0.0 123.8 %layer.1 = bf16[64,2048]{1,0:T(8,128)(2,1)} custom-call(bf16[64,2048]{1,0:T(8,128)(2,1)} %resid_ref.1, bf16[256,256]{1,0:T(8,128)(2,1)} %q_ref.1, bf16[256,256]{1,0:T(8,128)(2,1)} %k_ref.1, bf16[256,256]{1,0:T(8,128)(2,1)} %v_ref.1, f32[4,1024]{1,0:T(4,128)} %bitcast.2, f32[1,2048]{1,0:T(1,128)} %bitcast.3, bf16[1024,2048]{1,0:T(8,128)(2,1)} %w_out_ref.1, ...), custom_call_target="tpu_custom_call" | custom-call | tf_op jit(solution)/shard_map/layer/pallas_call | solution.py:503
  123.8 1.7 %copy.12 = bf16[64,2048]{1,0:T(8,128)(2,1)} copy(bf16[64,2048]{1,0:T(8,128)(2,1)} %layer.1) | data formatting | bytes 524288

commit v5 on v4

--- a/solution.py
+++ b/solution.py
@@ -216,8 +216,7 @@
     def send_weight(mat, dst):
         sized(dst, lambda skip: weight_out(mat, dst, skip).start())
 
-    for mat in range(2):
-        each(0, s, lambda i, mat=mat: send_weight(mat, s - 1 - i))
+    each(0, s, lambda i: send_weight(0, s - 1 - i))
 
     if dup:
 
@@ -352,10 +351,10 @@
     pl.when(s < ns - 2)(lambda: pl.semaphore_wait(go, 1))
     row_far(far).start()
     row_z(s, near).start()
-    for mat in range(2):
+    for mat in range(3):
         each(s + 1, ns, lambda i, mat=mat: send_weight(mat, i))
-    each(0, s, lambda i: send_weight(2, s - 1 - i))
-    each(s + 1, ns, lambda i: send_weight(2, i))
+        if mat:
+            each(0, s, lambda i, mat=mat: send_weight(mat, s - 1 - i))
     spread(s)
 
     def take_far():
@@ -367,18 +366,20 @@
         row_z(src, near).wait_recv()
         spread(src)
 
-    for mat in range(2):
-        each(s + 1, ns, lambda i, mat=mat: pass_on(mat, i))
+    def pass_all(mat):
+        each(s + 1, ns, lambda i: pass_on(mat, i))
+        each(0, s, lambda i: pass_on(mat, s - 1 - i))
+
+    each(s + 1, ns, lambda i: pass_on(0, i))
     relay(s)
-    pl.when(s >= 2)(take_far)
-    for mat in range(2):
-        each(0, s, lambda i, mat=mat: pass_on(mat, s - 1 - i))
-    pl.when(s < 2)(take_far)
+    take_far()
     take(near)
     relay(far)
     take(cross)
     relay(near)
-
+    each(0, s, lambda i: pass_on(0, s - 1 - i))
+    relay(cross)
+    pass_all(1)
     for copy in copies[1:]:
         copy.wait()
 
@@ -399,11 +400,8 @@
         up = jnp.dot(a, wu[...], preferred_element_type=F32)
         hidden[src] = jnp.where(fresh, gate / (1.0 + jnp.exp(-gate)) * up, 0.0).astype(BF16)
 
-    each(0, ns - 1, lambda k: hide(xor(s, k)))
-    each(s + 1, ns, lambda i: pass_on(2, i))
-    each(0, s, lambda i: pass_on(2, s - 1 - i))
-    relay(cross)
-    hide(cross)
+    each(0, ns, lambda k: hide(xor(s, k)))
+    pass_all(2)
     twin_in(2)
 
     def sum_c(d):

time: 126 us -> 150 us (1.19)
  Pallas kernels: 124 us -> 148 us
    pallas_call x1, Pallas kernels: 124 us -> 148 us  [fused(): pl.pallas_call(functools.partial(layer_kernel, (ns, nt, chunk)), out_shap...]
where the time goes in v5:
time: 150 us; the launch traced here: 149 us
  Pallas kernels  148 us (99%)
  local copies, waits for them, and re-layouts  1.67 us (1%)
    pallas_call x1, Pallas kernels, fused(): pl.pallas_call(functools.partial(layer_kernel, (ns, nt, chunk)), out_shap...  148 us

profile of v5, /device:TPU:0, one launch (start us, length us, event | category | flops | bytes accessed | tf_op | source)
XLA Modules:
  0.0 149.2 jit_solution(6228463274241825922)
XLA Ops:
  0.0 147.5 %layer.1 = bf16[64,2048]{1,0:T(8,128)(2,1)} custom-call(bf16[64,2048]{1,0:T(8,128)(2,1)} %resid_ref.1, bf16[256,256]{1,0:T(8,128)(2,1)} %q_ref.1, bf16[256,256]{1,0:T(8,128)(2,1)} %k_ref.1, bf16[256,256]{1,0:T(8,128)(2,1)} %v_ref.1, f32[4,1024]{1,0:T(4,128)} %bitcast.2, f32[1,2048]{1,0:T(1,128)} %bitcast.3, bf16[1024,2048]{1,0:T(8,128)(2,1)} %w_out_ref.1, ...), custom_call_target="tpu_custom_call" | custom-call | tf_op jit(solution)/shard_map/layer/pallas_call | solution.py:501
  147.5 1.7 %copy.12 = bf16[64,2048]{1,0:T(8,128)(2,1)} copy(bf16[64,2048]{1,0:T(8,128)(2,1)} %layer.1) | data formatting | bytes 524288

commit v6 on v4

--- a/solution.py
+++ b/solution.py
@@ -377,7 +377,10 @@
     take(near)
     relay(far)
     take(cross)
+    each(s + 1, ns, lambda i: pass_on(2, i))
+    each(0, s, lambda i: pass_on(2, s - 1 - i))
     relay(near)
+    relay(cross)
 
     for copy in copies[1:]:
         copy.wait()
@@ -399,11 +402,7 @@
         up = jnp.dot(a, wu[...], preferred_element_type=F32)
         hidden[src] = jnp.where(fresh, gate / (1.0 + jnp.exp(-gate)) * up, 0.0).astype(BF16)
 
-    each(0, ns - 1, lambda k: hide(xor(s, k)))
-    each(s + 1, ns, lambda i: pass_on(2, i))
-    each(0, s, lambda i: pass_on(2, s - 1 - i))
-    relay(cross)
-    hide(cross)
+    each(0, ns, lambda k: hide(xor(s, k)))
     twin_in(2)
 
     def sum_c(d):

time: 126 us -> 119 us (0.944)
  Pallas kernels: 124 us -> 117 us
    pallas_call x1, Pallas kernels: 124 us -> 117 us  [fused(): pl.pallas_call(functools.partial(layer_kernel, (ns, nt, chunk)), out_shap...]
where the time goes in v6:
time: 119 us
  Pallas kernels  117 us (98%)
  local copies, waits for them, and re-layouts  1.67 us (1%)
    pallas_call x1, Pallas kernels, fused(): pl.pallas_call(functools.partial(layer_kernel, (ns, nt, chunk)), out_shap...  117 us

profile of v6, /device:TPU:0, one launch (start us, length us, event | category | flops | bytes accessed | tf_op | source)
XLA Modules:
  0.0 118.9 jit_solution(13275806223400138188)
XLA Ops:
  0.0 117.3 %layer.1 = bf16[64,2048]{1,0:T(8,128)(2,1)} custom-call(bf16[64,2048]{1,0:T(8,128)(2,1)} %resid_ref.1, bf16[256,256]{1,0:T(8,128)(2,1)} %q_ref.1, bf16[256,256]{1,0:T(8,128)(2,1)} %k_ref.1, bf16[256,256]{1,0:T(8,128)(2,1)} %v_ref.1, f32[4,1024]{1,0:T(4,128)} %bitcast.2, f32[1,2048]{1,0:T(1,128)} %bitcast.3, bf16[1024,2048]{1,0:T(8,128)(2,1)} %w_out_ref.1, ...), custom_call_target="tpu_custom_call" | custom-call | tf_op jit(solution)/shard_map/layer/pallas_call | solution.py:502
  117.3 1.7 %copy.12 = bf16[64,2048]{1,0:T(8,128)(2,1)} copy(bf16[64,2048]{1,0:T(8,128)(2,1)} %layer.1) | data formatting | bytes 524288

commit v7 on v6

--- a/solution.py
+++ b/solution.py
@@ -375,10 +375,10 @@
         each(0, s, lambda i, mat=mat: pass_on(mat, s - 1 - i))
     pl.when(s < 2)(take_far)
     take(near)
-    relay(far)
     take(cross)
     each(s + 1, ns, lambda i: pass_on(2, i))
     each(0, s, lambda i: pass_on(2, s - 1 - i))
+    relay(far)
     relay(near)
     relay(cross)
 

time: 119 us -> 119 us (level)
  no operation moved by 1% of the time
where the time goes in v7:
time: 119 us
  Pallas kernels  117 us (98%)
  local copies, waits for them, and re-layouts  1.67 us (1%)
    pallas_call x1, Pallas kernels, fused(): pl.pallas_call(functools.partial(layer_kernel, (ns, nt, chunk)), out_shap...  117 us

profile of v7, /device:TPU:0, one launch (start us, length us, event | category | flops | bytes accessed | tf_op | source)
XLA Modules:
  0.0 118.9 jit_solution(5507246758006385868)
XLA Ops:
  0.0 117.3 %layer.1 = bf16[64,2048]{1,0:T(8,128)(2,1)} custom-call(bf16[64,2048]{1,0:T(8,128)(2,1)} %resid_ref.1, bf16[256,256]{1,0:T(8,128)(2,1)} %q_ref.1, bf16[256,256]{1,0:T(8,128)(2,1)} %k_ref.1, bf16[256,256]{1,0:T(8,128)(2,1)} %v_ref.1, f32[4,1024]{1,0:T(4,128)} %bitcast.2, f32[1,2048]{1,0:T(1,128)} %bitcast.3, bf16[1024,2048]{1,0:T(8,128)(2,1)} %w_out_ref.1, ...), custom_call_target="tpu_custom_call" | custom-call | tf_op jit(solution)/shard_map/layer/pallas_call | solution.py:502
  117.3 1.7 %copy.12 = bf16[64,2048]{1,0:T(8,128)(2,1)} copy(bf16[64,2048]{1,0:T(8,128)(2,1)} %layer.1) | data formatting | bytes 524288
